TPU v7x, 32 devices: a whole 2x2x4 slice. The times are simulated.
32 devices in a mesh: fs: 16 (over z, x, core), tp: 2 (over y).
Axes of the slice: x: 2, y: 2, z: 4, core: 2. Of those that a mesh axis runs over, the one named last changes fastest.
Arguments:
- normed_input: bfloat16 [8192, 2048], P('fs'), may hold values from -6 to 6
- value_cotangent: bfloat16 [8192, 2048], P('fs', 'tp'), may hold values from -6 to 6
- gated_output: bfloat16 [8192, 2048], P('fs', 'tp'), may hold values from -6 to 6
- layer_cotangent: bfloat16 [8192, 2048], P('fs'), may hold values from -6 to 6
- factor_value: bfloat16 [2048, 256], P('fs'), may hold values from -4 to 4, as said below
- factor_output: bfloat16 [2048, 256], P('fs'), may hold values from -4 to 4, as said below
- weight_value: float32 [2048, 2048], P('fs', 'tp'), may hold values from -0.125 to 0.125
- weight_output: float32 [2048, 2048], P('tp', 'fs'), may hold values from -0.125 to 0.125
- first_value: float32 [256, 2048], P('fs', 'tp'), may hold values from -2048 to 2048
- second_value: float32 [256, 2048], P('fs', 'tp'), may hold values from 32768 to 524288
- first_output: float32 [256, 2048], P('fs', 'tp'), may hold values from -2048 to 2048
- second_output: float32 [256, 2048], P('fs', 'tp'), may hold values from 32768 to 524288
Outputs:
- step_value: float32 [2048, 2048], P('fs', 'tp')
- step_output: float32 [2048, 2048], P('tp', 'fs')
- next_weight_value: float32 [2048, 2048], P('fs', 'tp')
- next_weight_output: float32 [2048, 2048], P('tp', 'fs')
- next_first_value: float32 [256, 2048], P('fs', 'tp')
- next_second_value: float32 [256, 2048], P('fs', 'tp')
- next_first_output: float32 [256, 2048], P('fs', 'tp')
- next_second_output: float32 [256, 2048], P('fs', 'tp')
- copy_value: bfloat16 [2048, 2048], P(None, 'tp')
- copy_output: bfloat16 [2048, 2048], P('tp')
Inputs may be any that keep to these rules, and one draw needn't show every extreme that they name: factor_value has full rank. factor_output has full rank.
All inputs are finite; a program needn't handle non-finite values.
Results may differ from a plain program's by a relative error of at most 0.0039.
Values may be sent and summed in bfloat16 or wider, within the bound.
A program may use at most 64 MiB of HBM per device.

v0:
```python
import functools

import jax
import jax.numpy as jnp
from jax import lax
from jax.experimental import pallas as pl
from jax.experimental.pallas import tpu as pltpu
from jax.sharding import PartitionSpec as P

CORES = 2

D = 2048
WIDTH = 2048


def gram_times(gram_matrix, directions):
    gram_high = gram_matrix.astype(jnp.bfloat16)
    gram_low = (gram_matrix - gram_high.astype(jnp.float32)).astype(jnp.bfloat16)
    return jnp.dot(gram_high, directions, preferred_element_type=jnp.float32) + jnp.dot(
        gram_low, directions, preferred_element_type=jnp.float32
    )


def body(
    normed_input,
    value_cotangent,
    gated_output,
    layer_cotangent,
    factor_value,
    factor_output,
    weight_value,
    weight_output,
    first_value,
    second_value,
    first_output,
    second_output,
):
    col_count = value_cotangent.shape[1]
    inner = (((0,), (0,)), ((), ()))
    pieces = (
        lax.all_gather(factor_value, "fs", axis=0, tiled=True),
        lax.all_gather(factor_output, "fs", axis=0, tiled=True),
    )
    piece_value, piece_output = pieces
    span_input = normed_input
    span_cotan = layer_cotangent
    gram_value = lax.dot_general(pieces[0], pieces[0], inner, preferred_element_type=jnp.float32)
    gram_output = lax.dot_general(pieces[1], pieces[1], inner, preferred_element_type=jnp.float32)
    projected_input = jnp.dot(span_input, piece_value, preferred_element_type=jnp.float32).astype(
        jnp.bfloat16
    )
    projected_cotangent = jnp.dot(
        span_cotan, piece_output, preferred_element_type=jnp.float32
    ).astype(jnp.bfloat16)
    span_input = projected_input
    span_cotan = projected_cotangent
    term_value = lax.dot_general(
        span_input, value_cotangent, inner, preferred_element_type=jnp.float32
    )
    term_output = lax.dot_general(
        span_cotan, gated_output, inner, preferred_element_type=jnp.float32
    )
    low_rank = lax.psum_scatter(
        jnp.concatenate([term_value, term_output], axis=1), "fs", scatter_dimension=0, tiled=True
    )
    low_value = low_rank[:, :col_count]
    low_output = low_rank[:, col_count:]
    next_first_value = 0.9 * first_value + 0.1 * low_value
    next_second_value = 0.95 * second_value + 0.05 * low_value * low_value
    next_first_output = 0.9 * first_output + 0.1 * low_output
    next_second_output = 0.95 * second_output + 0.05 * low_output * low_output
    direction_value = (next_first_value * lax.rsqrt(next_second_value)).astype(jnp.bfloat16)
    direction_output = (next_first_output * lax.rsqrt(next_second_output)).astype(jnp.bfloat16)
    gathered_value, gathered_output = (
        lax.all_gather(direction_value, "fs", axis=0, tiled=True),
        lax.all_gather(direction_output, "fs", axis=0, tiled=True),
    )
    update_value = jnp.dot(factor_value, gathered_value, preferred_element_type=jnp.float32)
    update_output = lax.dot_general(
        gathered_output, factor_output, (((0,), (1,)), ((), ())), preferred_element_type=jnp.float32
    )
    square_value = jnp.sum(
        gathered_value.astype(jnp.float32) * gram_times(gram_value, gathered_value)
    )
    square_output = jnp.sum(
        gathered_output.astype(jnp.float32) * gram_times(gram_output, gathered_output)
    )
    total_value, total_output = lax.psum((square_value, square_output), "tp")
    entries = D * WIDTH
    step_value = update_value * lax.rsqrt(total_value / entries + 1e-06)
    step_output = update_output * lax.rsqrt(total_output / entries + 1e-06)
    next_weight_value = weight_value - 0.02 * step_value
    next_weight_output = weight_output - 0.02 * step_output
    half_value = next_weight_value.astype(jnp.bfloat16)
    half_output = next_weight_output.astype(jnp.bfloat16)
    copy_value, copy_output = (
        lax.all_gather(half_value, "fs", axis=0, tiled=True),
        lax.all_gather(half_output, "fs", axis=1, tiled=True),
    )
    return (
        step_value,
        step_output,
        next_weight_value,
        next_weight_output,
        next_first_value,
        next_second_value,
        next_first_output,
        next_second_output,
        copy_value,
        copy_output,
    )


class Relay:
    def __init__(self, place, block, send_sem, recv_sem):
        self.z, self.x, self.core, self.depth, self.width = place
        self.block, self.send_sem, self.recv_sem = block, send_sem, recv_sem
        self.pending = []

    def index(self, shift, x, core):
        z = lax.rem(self.z + shift, self.depth)
        return (z * self.width + x) * CORES + core

    def copy(self, origin, target, slot):
        return pltpu.make_async_remote_copy(
            src_ref=self.block(origin),
            dst_ref=self.block(origin),
            send_sem=self.send_sem.at[slot],
            recv_sem=self.recv_sem.at[origin],
            device_id={"fs": target},
            device_id_type=pl.DeviceIdType.MESH,
        )

    def send(self, origin, target):
        copy = self.copy(origin, target, len(self.pending))
        copy.start()
        self.pending.append(copy)

    def arrived(self, origin):
        self.copy(origin, self.index(0, self.x, 1 - self.core), 0).wait_recv()

    def over_x(self, origin):
        self.send(origin, self.index(0, 1 - self.x, self.core))

    def over_core(self, origin):
        self.send(origin, self.index(0, self.x, 1 - self.core))

    def order(self):
        shifts = []
        for hop in range(1, self.depth // 2 + 1):
            for shift in (hop, self.depth - hop):
                if shift not in shifts:
                    shifts.append(shift)
        return shifts

    def begin(self):
        own = self.index(0, self.x, self.core)
        for shift in self.order():
            self.send(own, self.index(shift, self.x, self.core))
        self.over_x(own)
        self.over_core(own)

    def along_z(self, shift):
        origin = self.index(shift, self.x, self.core)
        self.arrived(origin)
        self.over_x(origin)
        self.over_core(origin)

    def across(self, shift):
        origin = self.index(shift, 1 - self.x, self.core)
        self.arrived(origin)
        self.over_core(origin)

    def middle(self):
        lagged = [0]
        for shift in self.order():
            yield functools.partial(self.along_z, shift)
            lagged.append(shift)
            if len(lagged) > 1:
                yield functools.partial(self.across, lagged.pop(0))
        for shift in lagged:
            yield functools.partial(self.across, shift)

    def finish(self):
        for shift in [0] + self.order():
            for x in (self.x, 1 - self.x):
                self.arrived(self.index(shift, x, 1 - self.core))
        for copy in self.pending:
            copy.wait_send()


def next_moments(first, second, low):
    return 0.9 * first + 0.1 * low, 0.95 * second + 0.05 * low * low


def fused(
    fs_size,
    tp_size,
    input_hbm,
    value_hbm,
    gated_hbm,
    layer_hbm,
    factor_value_hbm,
    factor_output_hbm,
    weight_value_ref,
    weight_output_ref,
    first_value_ref,
    second_value_ref,
    first_output_ref,
    second_output_ref,
    low_ref,
    directions,
    factors,
    scale_ref,
    wide_value_ref,
    wide_output_ref,
    stream,
    cotan,
    projected,
    terms,
    paired,
    outgoing,
    incoming,
    totals,
    load_sem,
    pair_send,
    pair_recv,
    sum_send,
    sum_recv,
    total_send,
    total_recv,
    relay_send,
    relay_recv,
):
    fs, tp = lax.axis_index("fs"), lax.axis_index("tp")
    width = tp_size
    chips = fs_size // CORES
    depth = chips // width
    core, chip = lax.rem(fs, CORES), fs // CORES
    x, z = lax.rem(chip, width), chip // width
    place = (z, x, core, depth, width)
    partner = chip * CORES + 1 - core
    mesh_id = pl.DeviceIdType.MESH
    rows = factor_value_hbm.shape[0]
    tokens = input_hbm.shape[0]
    cols = value_hbm.shape[1]
    ranks = first_value_ref.shape[0]
    everyone = [(a, b) for a in range(fs_size) for b in range(tp_size)][1:]

    own_rows = pl.ds(pl.multiple_of(fs * rows, rows), rows)
    loads = [
        pltpu.make_async_copy(source, target, load_sem.at[slot])
        for slot, (source, target) in enumerate(
            (
                (factor_value_hbm, factors.at[0, own_rows]),
                (factor_output_hbm, factors.at[1, own_rows]),
                (input_hbm, stream.at[0]),
                (layer_hbm, stream.at[1]),
                (value_hbm, cotan.at[0]),
                (gated_hbm, cotan.at[1]),
            )
        )
    ]
    for load in loads:
        load.start()

    barrier = pltpu.get_barrier_semaphore()
    for a, b in everyone:
        pl.semaphore_signal(
            barrier,
            inc=1,
            device_id={"fs": lax.rem(fs + a, fs_size), "tp": lax.rem(tp + b, tp_size)},
            device_id_type=mesh_id,
        )
    loads[0].wait()
    loads[1].wait()
    pl.semaphore_wait(barrier, len(everyone))

    def row_block(ref, size, lead=False):
        def block(origin):
            span = pl.ds(pl.multiple_of(origin * size, size), size)
            return ref.at[:, span] if lead else ref.at[span]

        return block

    half = cols // 2

    def rows_part(part):
        def block(origin):
            span = pl.ds(pl.multiple_of(origin * rows, rows), rows)
            return wide_value_ref.at[span, part * half : (part + 1) * half]

        return block

    def columns_part(part):
        def block(origin):
            span = pl.ds(pl.multiple_of(origin * rows, rows), rows)
            return wide_output_ref.at[part * half : (part + 1) * half, span]

        return block

    gathers = (
        row_block(factors, rows, True),
        row_block(directions, ranks),
        rows_part(0),
        rows_part(1),
        columns_part(0),
        columns_part(1),
    )
    relays = [
        Relay(place, block, relay_send.at[slot], relay_recv.at[slot])
        for slot, block in enumerate(gathers)
    ]

    relays[0].begin()
    wide_value_ref[own_rows, :] = weight_value_ref[...].astype(jnp.bfloat16)
    wide_output_ref[:, own_rows] = weight_output_ref[...].astype(jnp.bfloat16)
    for step in relays[0].middle():
        step()
    relays[2].begin()
    relays[0].finish()
    for load in loads[2:]:
        load.wait()

    tile = 128
    for kind in range(2):

        @pl.loop(0, tokens // tile)
        def _(step, kind=kind):
            span = pl.ds(pl.multiple_of(step * tile, tile), tile)
            projected[kind, span] = jnp.dot(
                stream[kind, span], factors[kind], preferred_element_type=jnp.float32
            ).astype(jnp.bfloat16)

    width_tile = 256
    for kind in range(2):

        @pl.loop(0, cols // width_tile)
        def _(step, kind=kind):
            span = pl.ds(pl.multiple_of(step * width_tile, width_tile), width_tile)
            term = lax.dot_general(
                projected[kind],
                cotan[kind, :, span],
                (((0,), (0,)), ((), ())),
                preferred_element_type=jnp.float32,
            )
            target = pl.ds(pl.multiple_of(kind * cols + step * width_tile, width_tile), width_tile)
            terms[:, :, :, target] = term.reshape(chips, CORES, ranks, width_tile)

    pairs = []
    for shift in list(range(1, chips)) + [0]:
        c = lax.rem(chip + shift, chips)
        copy = pltpu.make_async_remote_copy(
            src_ref=terms.at[c, 1 - core],
            dst_ref=paired.at[c],
            send_sem=pair_send.at[shift],
            recv_sem=pair_recv.at[c],
            device_id={"fs": partner},
            device_id_type=mesh_id,
        )
        copy.start()
        pairs.append(copy)
    sums = []
    for shift in range(1, chips):
        c = lax.rem(chip + shift, chips)
        pairs[shift - 1].wait_recv()
        outgoing[c] = (terms[c, core] + paired[c]).astype(jnp.bfloat16)
        copy = pltpu.make_async_remote_copy(
            src_ref=outgoing.at[c],
            dst_ref=incoming.at[chip],
            send_sem=sum_send.at[shift],
            recv_sem=sum_recv.at[chip],
            device_id={"fs": c * CORES + core},
            device_id_type=mesh_id,
        )
        copy.start()
        sums.append(copy)
    for step in relays[2].middle():
        step()
    relays[3].begin()
    pairs[-1].wait_recv()
    low = terms[chip, core] + paired[chip]
    for shift in range(1, chips):
        c = lax.rem(chip + chips - shift, chips)
        pltpu.make_async_remote_copy(
            src_ref=outgoing.at[c],
            dst_ref=incoming.at[c],
            send_sem=sum_send.at[shift],
            recv_sem=sum_recv.at[c],
            device_id={"fs": c * CORES + core},
            device_id_type=mesh_id,
        ).wait_recv()
        low = low + incoming[c].astype(jnp.float32)

    own_ranks = pl.ds(pl.multiple_of(fs * ranks, ranks), ranks)
    low_ref[...] = low
    moments = ((first_value_ref, second_value_ref), (first_output_ref, second_output_ref))
    for kind, (first_ref, second_ref) in enumerate(moments):
        part = low[:, kind * cols : (kind + 1) * cols]
        next_first, next_second = next_moments(first_ref[...], second_ref[...], part)
        directions[own_ranks, kind * cols : (kind + 1) * cols] = (
            next_first * lax.rsqrt(next_second)
        ).astype(jnp.bfloat16)
    relays[1].begin()
    for first, second in zip(relays[1].middle(), relays[3].middle()):
        first()
        second()
    relays[4].begin()
    relays[5].begin()
    relays[1].finish()

    me = fs * tp_size + tp
    for kind in range(2):
        square = jnp.zeros((8, 128), jnp.float32)
        for start in range(0, cols, width_tile):
            update = jnp.dot(
                factors[kind, own_rows],
                directions[:, kind * cols + start : kind * cols + start + width_tile],
                preferred_element_type=jnp.float32,
            )
            fold = jnp.sum((update * update).reshape(rows // 8, 8, width_tile), axis=0)
            for lane in range(0, width_tile, 128):
                square = square + fold[:, lane : lane + 128]
        totals[me, kind] = square
    shares = []
    for slot, (a, b) in enumerate(everyone):
        copy = pltpu.make_async_remote_copy(
            src_ref=totals.at[me],
            dst_ref=totals.at[me],
            send_sem=total_send.at[slot],
            recv_sem=total_recv.at[me],
            device_id={"fs": lax.rem(fs + a, fs_size), "tp": lax.rem(tp + b, tp_size)},
            device_id_type=mesh_id,
        )
        copy.start()
        shares.append(copy)
    for first, second in zip(relays[4].middle(), relays[5].middle()):
        first()
        second()
    for a, b in everyone:
        other_fs, other_tp = lax.rem(fs + a, fs_size), lax.rem(tp + b, tp_size)
        other = other_fs * tp_size + other_tp
        pltpu.make_async_remote_copy(
            src_ref=totals.at[other],
            dst_ref=totals.at[other],
            send_sem=total_send.at[0],
            recv_sem=total_recv.at[other],
            device_id={"fs": other_fs, "tp": other_tp},
            device_id_type=mesh_id,
        ).wait_recv()
    entries = rows * fs_size * cols * tp_size
    for kind in range(2):
        total = jnp.sum(jnp.sum(totals[:, kind], axis=0), keepdims=True)
        scale = lax.rsqrt(total / entries + 1e-06)
        scale_ref[kind] = jnp.broadcast_to(scale, scale_ref.shape[1:])
    for relay in relays[2:]:
        relay.finish()
    for copy in pairs + sums + shares:
        copy.wait_send()


def apply(
    low_ref,
    directions,
    factors,
    scale_ref,
    wide_value_ref,
    wide_output_ref,
    factor_value_ref,
    factor_output_ref,
    weight_value_ref,
    weight_output_ref,
    first_value_ref,
    second_value_ref,
    first_output_ref,
    second_output_ref,
    step_value_ref,
    step_output_ref,
    next_weight_value_ref,
    next_weight_output_ref,
    next_first_value_ref,
    next_second_value_ref,
    next_first_output_ref,
    next_second_output_ref,
    copy_value_ref,
    copy_output_ref,
    turned,
):
    cols = weight_value_ref.shape[1]
    scale_value, scale_output = scale_ref[0, :1, :1], scale_ref[1, :1, :1]
    last = (((1,), (1,)), ((), ()))

    def update_value(factor):
        return jnp.dot(factor, directions[:, :cols], preferred_element_type=jnp.float32)

    def update_output(factor):
        return lax.dot_general(turned[...], factor, last, preferred_element_type=jnp.float32)

    @pl.when(pl.program_id(0) == 0)
    def _():
        turned[...] = directions[:, cols:].astype(jnp.float32).T.astype(jnp.bfloat16)
        moments = (
            (first_value_ref, second_value_ref, next_first_value_ref, next_second_value_ref),
            (first_output_ref, second_output_ref, next_first_output_ref, next_second_output_ref),
        )
        for kind, (first_ref, second_ref, next_first_ref, next_second_ref) in enumerate(moments):
            next_first_ref[...], next_second_ref[...] = next_moments(
                first_ref[...], second_ref[...], low_ref[:, kind * cols : (kind + 1) * cols]
            )
        step_value = update_value(factor_value_ref[...]) * scale_value
        step_value_ref[...] = step_value
        next_weight_value_ref[...] = weight_value_ref[...] - 0.02 * step_value
        step_output = update_output(factor_output_ref[...]) * scale_output
        step_output_ref[...] = step_output
        next_weight_output_ref[...] = weight_output_ref[...] - 0.02 * step_output

    copy_value_ref[...] = (
        wide_value_ref[...].astype(jnp.float32) - update_value(factors[0]) * (0.02 * scale_value)
    ).astype(jnp.bfloat16)
    copy_output_ref[...] = (
        wide_output_ref[...].astype(jnp.float32) - update_output(factors[1]) * (0.02 * scale_output)
    ).astype(jnp.bfloat16)


def fused_body(fs_size, tp_size, *args):
    tokens, model = args[0].shape
    cols = args[1].shape[1]
    rows, rank = args[4].shape
    ranks = args[8].shape[0]
    chips = fs_size // CORES
    f32, bf16 = jnp.float32, jnp.bfloat16
    vmem, anywhere = pl.BlockSpec(memory_space=pltpu.VMEM), pl.BlockSpec(memory_space=pl.ANY)
    shape = jax.ShapeDtypeStruct
    hops = chips // tp_size - 1 + chips // tp_size + chips
    dma = pltpu.SemaphoreType.DMA
    gathered = pl.pallas_call(
        functools.partial(fused, fs_size, tp_size),
        out_shape=[
            shape((ranks, 2 * cols), f32),
            shape((rank, 2 * cols), bf16),
            shape((2, model, rank), bf16),
            shape((2, 8, 128), f32),
            shape((model, cols), bf16),
            shape((cols, model), bf16),
        ],
        in_specs=[anywhere] * 6 + [vmem] * 6,
        out_specs=[vmem] * 6,
        scratch_shapes=[
            pltpu.VMEM((2, tokens, model), bf16),
            pltpu.VMEM((2, tokens, cols), bf16),
            pltpu.VMEM((2, tokens, rank), bf16),
            pltpu.VMEM((chips, CORES, ranks, 2 * cols), f32),
            pltpu.VMEM((chips, ranks, 2 * cols), f32),
            pltpu.VMEM((chips, ranks, 2 * cols), bf16),
            pltpu.VMEM((chips, ranks, 2 * cols), bf16),
            pltpu.VMEM((fs_size * tp_size, 2, 8, 128), f32),
            dma((6,)),
            dma((chips,)),
            dma((chips,)),
            dma((chips,)),
            dma((chips,)),
            dma((fs_size * tp_size,)),
            dma((fs_size * tp_size,)),
            dma((6, hops)),
            dma((6, fs_size)),
        ],
        compiler_params=pltpu.CompilerParams(
            collective_id=0, has_side_effects=True, vmem_limit_bytes=60 * 1024 * 1024
        ),
    )(*args)

    tile = 2 * rows

    def whole(array):
        return pl.BlockSpec(array.shape, lambda i: (0,) * len(array.shape))

    by_rows = pl.BlockSpec((tile, cols), lambda i: (i, 0))
    by_columns = pl.BlockSpec((cols, tile), lambda i: (0, i))
    own = [shape((rows, cols), f32), shape((cols, rows), f32)] * 2 + [shape((ranks, cols), f32)] * 4
    low, directions, factors, scales = gathered[:4]
    return pl.pallas_call(
        apply,
        grid=(model // tile,),
        out_shape=own + [shape((model, cols), bf16), shape((cols, model), bf16)],
        in_specs=[
            whole(low),
            whole(directions),
            pl.BlockSpec((2, tile, rank), lambda i: (0, i, 0)),
            whole(scales),
            by_rows,
            by_columns,
        ]
        + [whole(array) for array in args[4:]],
        out_specs=[whole(array) for array in own] + [by_rows, by_columns],
        scratch_shapes=[pltpu.VMEM((cols, rank), bf16)],
        compiler_params=pltpu.CompilerParams(vmem_limit_bytes=60 * 1024 * 1024),
    )(*gathered, *args[4:])


def solution(mesh):
    fs_size, tp_size = mesh.shape["fs"], mesh.shape["tp"]
    placed = (
        P("fs", None),
        P("fs", "tp"),
        P("fs", "tp"),
        P("fs", None),
        P("fs", None),
        P("fs", None),
        P("fs", "tp"),
        P("tp", "fs"),
        P("fs", "tp"),
        P("fs", "tp"),
        P("fs", "tp"),
        P("fs", "tp"),
    )
    chips = fs_size // CORES
    tiled = tp_size == 2 and fs_size == 16 and chips % tp_size == 0
    return jax.shard_map(
        functools.partial(fused_body, fs_size, tp_size) if tiled else body,
        mesh=mesh,
        in_specs=placed,
        out_specs=(
            P("fs", "tp"),
            P("tp", "fs"),
            P("fs", "tp"),
            P("tp", "fs"),
            P("fs", "tp"),
            P("fs", "tp"),
            P("fs", "tp"),
            P("fs", "tp"),
            P(None, "tp"),
            P("tp", None),
        ),
        check_vma=False,
    )
```

profile of v0, /device:TPU:9, one launch (start us, length us, event | category | flops | bytes accessed | tf_op | source)
XLA Modules:
  0.0 129.7 jit_solution(12877227673334135607)
XLA Ops:
  0.6 117.0 %shard_map.195 = (f32[16,2048]{1,0:T(8,128)}, bf16[256,2048]{1,0:T(8,128)(2,1)}, bf16[2,2048,256]{2,1,0:T(8,128)(2,1)}, f32[2,8,128]{2,1,0:T(8,128)}, bf16[2048,...) custom-call(bf16[512,2048]{1,0:T(8,128)(2,1)} %input_hbm.1, bf16[512,1024]{1,0:T(8,128)(2,1)} %value_hbm.1, ...), custom_call_target="tpu_custom_call" | custom-call | tf_op jit(solution)/shard_map/pallas_call | solution.py:536
  117.7 12.1 %shard_map.196 = (f32[128,1024]{1,0:T(8,128)}, f32[1024,128]{1,0:T(8,128)}, f32[128,1024]{1,0:T(8,128)}, f32[1024,128]{1,0:T(8,128)}, f32[16,1024]{1,0:T(8,128)}...) custom-call(f32[16,2048]{1,0:T(8,128)} %get-tuple-element.16.low_ref, ...), custom_call_target="tpu_custom_call" | custom-call | tf_op jit(solution)/shard_map/pallas_call | solution.py:581
where the time goes:
time: 130 us
  Pallas kernels  129 us (99%)
    pallas_call x1, Pallas kernels, fused_body(): pl.pallas_call(functools.partial(fused, fs_size, tp_size), out_shape=[sha...  117 us
    pallas_call x1, Pallas kernels, fused_body(): pl.pallas_call(apply, grid=(model // tile,), out_shape=own + [shape((mode...  12.1 us

commit v1 on v0

v1 whole, which is shorter than its diff:
```python
import functools

import jax
import jax.numpy as jnp
from jax import lax
from jax.experimental import pallas as pl
from jax.experimental.pallas import tpu as pltpu
from jax.sharding import PartitionSpec as P

CORES = 2

D = 2048
WIDTH = 2048


def gram_times(gram_matrix, directions):
    gram_high = gram_matrix.astype(jnp.bfloat16)
    gram_low = (gram_matrix - gram_high.astype(jnp.float32)).astype(jnp.bfloat16)
    return jnp.dot(gram_high, directions, preferred_element_type=jnp.float32) + jnp.dot(
        gram_low, directions, preferred_element_type=jnp.float32
    )


def body(
    normed_input,
    value_cotangent,
    gated_output,
    layer_cotangent,
    factor_value,
    factor_output,
    weight_value,
    weight_output,
    first_value,
    second_value,
    first_output,
    second_output,
):
    col_count = value_cotangent.shape[1]
    inner = (((0,), (0,)), ((), ()))
    pieces = (
        lax.all_gather(factor_value, "fs", axis=0, tiled=True),
        lax.all_gather(factor_output, "fs", axis=0, tiled=True),
    )
    piece_value, piece_output = pieces
    span_input = normed_input
    span_cotan = layer_cotangent
    gram_value = lax.dot_general(pieces[0], pieces[0], inner, preferred_element_type=jnp.float32)
    gram_output = lax.dot_general(pieces[1], pieces[1], inner, preferred_element_type=jnp.float32)
    projected_input = jnp.dot(span_input, piece_value, preferred_element_type=jnp.float32).astype(
        jnp.bfloat16
    )
    projected_cotangent = jnp.dot(
        span_cotan, piece_output, preferred_element_type=jnp.float32
    ).astype(jnp.bfloat16)
    span_input = projected_input
    span_cotan = projected_cotangent
    term_value = lax.dot_general(
        span_input, value_cotangent, inner, preferred_element_type=jnp.float32
    )
    term_output = lax.dot_general(
        span_cotan, gated_output, inner, preferred_element_type=jnp.float32
    )
    low_rank = lax.psum_scatter(
        jnp.concatenate([term_value, term_output], axis=1), "fs", scatter_dimension=0, tiled=True
    )
    low_value = low_rank[:, :col_count]
    low_output = low_rank[:, col_count:]
    next_first_value = 0.9 * first_value + 0.1 * low_value
    next_second_value = 0.95 * second_value + 0.05 * low_value * low_value
    next_first_output = 0.9 * first_output + 0.1 * low_output
    next_second_output = 0.95 * second_output + 0.05 * low_output * low_output
    direction_value = (next_first_value * lax.rsqrt(next_second_value)).astype(jnp.bfloat16)
    direction_output = (next_first_output * lax.rsqrt(next_second_output)).astype(jnp.bfloat16)
    gathered_value, gathered_output = (
        lax.all_gather(direction_value, "fs", axis=0, tiled=True),
        lax.all_gather(direction_output, "fs", axis=0, tiled=True),
    )
    update_value = jnp.dot(factor_value, gathered_value, preferred_element_type=jnp.float32)
    update_output = lax.dot_general(
        gathered_output, factor_output, (((0,), (1,)), ((), ())), preferred_element_type=jnp.float32
    )
    square_value = jnp.sum(
        gathered_value.astype(jnp.float32) * gram_times(gram_value, gathered_value)
    )
    square_output = jnp.sum(
        gathered_output.astype(jnp.float32) * gram_times(gram_output, gathered_output)
    )
    total_value, total_output = lax.psum((square_value, square_output), "tp")
    entries = D * WIDTH
    step_value = update_value * lax.rsqrt(total_value / entries + 1e-06)
    step_output = update_output * lax.rsqrt(total_output / entries + 1e-06)
    next_weight_value = weight_value - 0.02 * step_value
    next_weight_output = weight_output - 0.02 * step_output
    half_value = next_weight_value.astype(jnp.bfloat16)
    half_output = next_weight_output.astype(jnp.bfloat16)
    copy_value, copy_output = (
        lax.all_gather(half_value, "fs", axis=0, tiled=True),
        lax.all_gather(half_output, "fs", axis=1, tiled=True),
    )
    return (
        step_value,
        step_output,
        next_weight_value,
        next_weight_output,
        next_first_value,
        next_second_value,
        next_first_output,
        next_second_output,
        copy_value,
        copy_output,
    )


def next_moments(first, second, low):
    return 0.9 * first + 0.1 * low, 0.95 * second + 0.05 * low * low


MESH = pl.DeviceIdType.MESH


class Sender:
    def __init__(self, sems):
        self.sems, self.pending = sems, []

    def send(self, source, target, recv_sem, device, when=None):
        copy = pltpu.make_async_remote_copy(
            src_ref=source,
            dst_ref=target,
            send_sem=self.sems.at[len(self.pending)],
            recv_sem=recv_sem,
            device_id=device,
            device_id_type=MESH,
        )
        self.guarded(copy.start, when)
        self.pending.append((copy, when))

    def guarded(self, action, when):
        if when is None:
            action()
        else:

            @pl.when(when)
            def _():
                action()

    def drain(self):
        for copy, when in self.pending:
            self.guarded(copy.wait_send, when)


def fused(
    fs_size,
    tp_size,
    input_hbm,
    value_hbm,
    gated_hbm,
    layer_hbm,
    factor_value_hbm,
    factor_output_hbm,
    weight_value_hbm,
    weight_output_hbm,
    first_value_hbm,
    second_value_hbm,
    first_output_hbm,
    second_output_hbm,
    moments,
    directions,
    turned,
    factors,
    scale_ref,
    wide_value,
    wide_output,
    stream,
    cotan,
    weight_value,
    weight_output,
    old,
    projection,
    flipped,
    terms,
    paired,
    out_x,
    in_x,
    out_z,
    in_z,
    totals,
    load_sem,
    send_sem,
    factor_recv,
    weight_recv,
    direction_recv,
    pair_recv,
    x_recv,
    z_recv,
    total_recv,
):
    fs, tp = lax.axis_index("fs"), lax.axis_index("tp")
    width = tp_size
    chips = fs_size // CORES
    depth = chips // width
    core, chip = lax.rem(fs, CORES), fs // CORES
    x, z = lax.rem(chip, width), chip // width
    rows, rank = factor_value_hbm.shape
    tokens = input_hbm.shape[0]
    cols = value_hbm.shape[1]
    ranks = first_value_hbm.shape[0]
    model = rows * fs_size
    last = depth - 1
    span = CORES * rows

    def index(z_at, x_at, core_at):
        return (z_at * width + x_at) * CORES + core_at

    def along_z(z_at):
        return {"fs": index(z_at, x, core)}

    over_x = {"fs": index(z, 1 - x, core)}
    over_core = {"fs": index(z, x, 1 - core)}
    over_y = {"tp": 1 - tp}
    beside = z + 1 - 2 * lax.rem(z, 2)
    mirror = last - z
    across = lax.rem(z + depth // 2, depth)
    others = (beside, mirror, across)
    middle = jnp.logical_and(z > 0, z < last)

    def block(ref, origin, size):
        return ref.at[pl.ds(pl.multiple_of(origin * size, size), size)]

    sources = (
        factor_value_hbm,
        factor_output_hbm,
        weight_value_hbm,
        weight_output_hbm,
        input_hbm,
        layer_hbm,
        value_hbm,
        gated_hbm,
        first_value_hbm,
        second_value_hbm,
        first_output_hbm,
        second_output_hbm,
    )
    targets = (
        block(factors.at[0], fs, rows),
        block(factors.at[1], fs, rows),
        weight_value,
        weight_output,
        stream.at[0],
        stream.at[1],
        cotan.at[0],
        cotan.at[1],
        old.at[0],
        old.at[1],
        old.at[2],
        old.at[3],
    )
    loads = [
        pltpu.make_async_copy(source, target, load_sem.at[slot])
        for slot, (source, target) in enumerate(zip(sources, targets))
    ]
    for load in loads:
        load.start()

    barrier = pltpu.get_barrier_semaphore()
    peers = [along_z(z_at) for z_at in others] + [over_x, over_core, over_y]
    for peer in peers:
        pl.semaphore_signal(barrier, inc=1, device_id=peer, device_id_type=MESH)
    loads[0].wait()
    loads[1].wait()
    pl.semaphore_wait(barrier, len(peers))

    sender = Sender(send_sem)

    def arrived(ref, recv_sem):
        pltpu.make_async_remote_copy(
            src_ref=ref,
            dst_ref=ref,
            send_sem=send_sem.at[0],
            recv_sem=recv_sem,
            device_id=over_core,
            device_id_type=MESH,
        ).wait_recv()

    def forward(ref, recv_sem, device, when=None):
        sender.send(ref, ref, recv_sem, device, when)

    mine, theirs = tp, 1 - tp

    def factor(kind, origin):
        return block(factors.at[kind], origin, rows), factor_recv.at[kind, origin]

    for z_at in others:
        forward(*factor(mine, fs), along_z(z_at))
    forward(*factor(mine, fs), over_x)
    forward(*factor(theirs, fs), over_x)
    forward(*factor(mine, fs), over_core)
    forward(*factor(theirs, fs), over_core)

    half_rows, half_cols = rows // 2, cols // 2

    def piece(part, origin):
        start = pl.multiple_of(origin * rows, rows)
        if part < 2:
            ref = wide_value.at[pl.ds(start + part * half_rows, half_rows)]
        else:
            ref = wide_output.at[pl.ds((part - 2) * half_cols, half_cols), pl.ds(start, rows)]
        return ref, weight_recv.at[part, origin]

    def piece_z(part, origin):
        forward(*piece(part, origin), along_z(beside))
        forward(*piece(part, origin), along_z(mirror), middle)
        forward(*piece(part, origin), along_z(across))

    beyond = along_z(jnp.clip(last * (z - 1), 0, last))

    def piece_arrives_z(part, x_at, cross):
        for z_at in others:
            ref, sem = piece(part, index(z_at, x_at, core))
            arrived(ref, sem)
            if z_at is across:
                forward(ref, sem, beyond, middle)
            if cross:
                forward(ref, sem, over_x)
            forward(ref, sem, over_core)

    def piece_arrives_x(part, z_at):
        ref, sem = piece(part, index(z_at, 1 - x, core))
        arrived(ref, sem)
        forward(ref, sem, over_core)

    loads[2].wait()
    loads[3].wait()
    own_rows = pl.ds(pl.multiple_of(fs * rows, rows), rows)
    wide_value[own_rows, :] = weight_value[...].astype(jnp.bfloat16)
    wide_output[:, own_rows] = weight_output[...].astype(jnp.bfloat16)
    piece_z(1, fs)
    piece_z(2, fs)

    for z_at in others:
        ref, sem = factor(mine, index(z_at, x, core))
        arrived(ref, sem)
        forward(ref, sem, over_x)
        forward(ref, sem, over_y)
        forward(ref, sem, over_core)
    for part in range(4):
        forward(*piece(part, fs), over_x)
    ref, sem = factor(theirs, index(z, 1 - x, core))
    arrived(ref, sem)
    forward(ref, sem, over_core)
    for z_at in (z,) + others:
        ref, sem = factor(mine, index(z_at, 1 - x, core))
        arrived(ref, sem)
        if z_at is not z:
            forward(ref, sem, over_y)
        forward(ref, sem, over_core)
    for load in loads[4:]:
        load.wait()

    def project(kind, z_at, x_at, first=False):
        arrived(*factor(kind, index(z_at, x_at, 1 - core)))
        part = pl.ds(pl.multiple_of((z_at * width + x_at) * span, span), span)
        product = jnp.dot(
            stream[kind, :, part], factors[kind, part], preferred_element_type=jnp.float32
        )
        projection[kind] = product if first else projection[kind] + product

    def from_y(z_at, x_at):
        ref, sem = factor(theirs, index(z_at, x_at, core))
        arrived(ref, sem)
        forward(ref, sem, over_core)

    project(mine, z, x, True)
    project(theirs, z, x, True)
    for z_at in others:
        project(mine, z_at, x)
    for z_at in others:
        from_y(z_at, x)
    for z_at in (z,) + others:
        project(mine, z_at, 1 - x)
    for z_at in others:
        from_y(z_at, 1 - x)
    for part in range(4):
        forward(*piece(part, fs), over_core)
    for z_at in others:
        project(theirs, z_at, x)
    for z_at in (z,) + others:
        project(theirs, z_at, 1 - x)

    width_tile = 256
    for kind in range(2):
        flipped[...] = projection[kind].T.astype(jnp.bfloat16)

        @pl.loop(0, cols // width_tile)
        def _(step, kind=kind):
            tile = pl.ds(pl.multiple_of(step * width_tile, width_tile), width_tile)
            term = jnp.dot(flipped[...], cotan[kind, :, tile], preferred_element_type=jnp.float32)
            target = pl.ds(pl.multiple_of(kind * cols + step * width_tile, width_tile), width_tile)
            terms[:, :, :, target] = term.reshape(chips, CORES, ranks, width_tile)

    far = others + (z,)
    for x_at in (1 - x, x):
        for z_at in far:
            to = z_at * width + x_at
            sender.send(terms.at[to, 1 - core], paired.at[to], pair_recv.at[to], over_core)

    def pair_sum(z_at, x_at):
        at = z_at * width + x_at
        arrived(paired.at[at], pair_recv.at[at])
        return terms[at, core] + paired[at]

    for z_at in far:
        out_x[z_at] = pair_sum(z_at, 1 - x).astype(jnp.bfloat16)
        sender.send(out_x.at[z_at], in_x.at[z_at], x_recv.at[z_at], over_x)
    piece_arrives_z(1, x, True)

    def column_sum(z_at):
        total = pair_sum(z_at, x)
        arrived(in_x.at[z_at], x_recv.at[z_at])
        return total + in_x[z_at].astype(jnp.float32)

    for z_at in others:
        out_z[z_at] = column_sum(z_at).astype(jnp.bfloat16)
        sender.send(out_z.at[z_at], in_z.at[z], z_recv.at[z], along_z(z_at))
    piece_z(3, fs)
    low = column_sum(z)
    for z_at in others:
        arrived(in_z.at[z_at], z_recv.at[z_at])
        low = low + in_z[z_at].astype(jnp.float32)

    own_ranks = pl.ds(pl.multiple_of(fs * ranks, ranks), ranks)
    for kind in range(2):
        part = low[:, kind * cols : (kind + 1) * cols]
        next_first, next_second = next_moments(old[2 * kind], old[2 * kind + 1], part)
        moments[2 * kind] = next_first
        moments[2 * kind + 1] = next_second
        directions[own_ranks, kind * cols : (kind + 1) * cols] = (
            next_first * lax.rsqrt(next_second)
        ).astype(jnp.bfloat16)

    def direction(origin):
        return block(directions, origin, ranks), direction_recv.at[origin]

    for z_at in others:
        forward(*direction(fs), along_z(z_at))
    forward(*direction(fs), over_x)
    forward(*direction(fs), over_core)
    for z_at in others:
        ref, sem = direction(index(z_at, x, core))
        arrived(ref, sem)
        forward(ref, sem, over_x)
        forward(ref, sem, over_core)
    piece_arrives_x(0, z)
    piece_z(0, fs)
    piece_z(0, index(z, 1 - x, core))
    piece_arrives_z(2, x, True)
    for z_at in (z,) + others:
        ref, sem = direction(index(z_at, 1 - x, core))
        arrived(ref, sem)
        forward(ref, sem, over_core)
    for z_at in (z,) + others:
        for x_at in (x, 1 - x):
            arrived(*direction(index(z_at, x_at, 1 - core)))

    tile = 256
    for kind in range(2):
        totals[tp, kind] = jnp.zeros((8, cols), jnp.float32)

        @pl.loop(0, model // tile)
        def _(step, kind=kind):
            update = jnp.dot(
                factors[kind, pl.ds(pl.multiple_of(step * tile, tile), tile)],
                directions[:, kind * cols : (kind + 1) * cols],
                preferred_element_type=jnp.float32,
            )
            totals[tp, kind] += jnp.sum((update * update).reshape(tile // 8, 8, cols), axis=0)

    sender.send(totals.at[tp], totals.at[tp], total_recv.at[tp], over_y)
    turned[...] = directions[:, cols:].astype(jnp.float32).T.astype(jnp.bfloat16)

    piece_arrives_z(3, x, True)
    for z_at in (z,) + others:
        piece_arrives_x(1, z_at)
    piece_arrives_z(0, x, False)
    piece_arrives_z(0, 1 - x, False)
    arrived(totals.at[1 - tp], total_recv.at[1 - tp])
    entries = model * cols * tp_size
    for kind in range(2):
        total = jnp.sum(totals[0, kind] + totals[1, kind], keepdims=True)
        scale = lax.rsqrt(total / entries + 1e-06)
        scale_ref[kind] = jnp.broadcast_to(scale, scale_ref.shape[1:])
    for part in (2, 3):
        for z_at in (z,) + others:
            piece_arrives_x(part, z_at)
    for part in range(4):
        for z_at in (z,) + others:
            for x_at in (x, 1 - x):
                arrived(*piece(part, index(z_at, x_at, 1 - core)))
    sender.drain()


def apply(
    moments,
    directions,
    turned,
    factors,
    scale_ref,
    wide_value,
    wide_output,
    weight_value_hbm,
    weight_output_hbm,
    step_value_hbm,
    step_output_hbm,
    next_weight_value_hbm,
    next_weight_output_hbm,
    next_first_value_hbm,
    next_second_value_hbm,
    next_first_output_hbm,
    next_second_output_hbm,
    copy_value_hbm,
    copy_output_hbm,
    weight_value,
    weight_output,
    step_value,
    step_output,
    next_value,
    next_output,
    copy_value,
    copy_output,
    load_sem,
    store_sem,
    value_sem,
    output_sem,
):
    rows, cols = weight_value_hbm.shape
    model = factors.shape[1]
    fs = lax.axis_index("fs")
    scale_value, scale_output = scale_ref[0, :1, :1], scale_ref[1, :1, :1]
    transposed = (((1,), (1,)), ((), ()))
    loads = [
        pltpu.make_async_copy(weight_value_hbm, weight_value, load_sem.at[0]),
        pltpu.make_async_copy(weight_output_hbm, weight_output, load_sem.at[1]),
    ]
    for load in loads:
        load.start()
    stores = []

    def store(source, target):
        copy = pltpu.make_async_copy(source, target, store_sem.at[len(stores)])
        copy.start()
        stores.append(copy)

    store(moments.at[0], next_first_value_hbm)
    store(moments.at[1], next_second_value_hbm)
    store(moments.at[2], next_first_output_hbm)
    store(moments.at[3], next_second_output_hbm)

    def update_value(factor):
        return jnp.dot(factor, directions[:, :cols], preferred_element_type=jnp.float32)

    def update_output(factor):
        return lax.dot_general(turned[...], factor, transposed, preferred_element_type=jnp.float32)

    tile = 256

    def value_copy(step):
        part = pl.ds(pl.multiple_of(step * tile, tile), tile)
        return pltpu.make_async_copy(
            copy_value.at[part], copy_value_hbm.at[part], value_sem.at[step]
        )

    def output_copy(step):
        part = pl.ds(pl.multiple_of(step * tile, tile), tile)
        return pltpu.make_async_copy(
            copy_output.at[:, part], copy_output_hbm.at[:, part], output_sem.at[step]
        )

    @pl.loop(0, model // tile)
    def _(step):
        part = pl.ds(pl.multiple_of(step * tile, tile), tile)
        copy_value[part] = (
            wide_value[part].astype(jnp.float32)
            - update_value(factors[0, part]) * (0.02 * scale_value)
        ).astype(jnp.bfloat16)
        value_copy(step).start()

    own_rows = pl.ds(pl.multiple_of(fs * rows, rows), rows)
    loads[0].wait()
    step = update_value(factors[0, own_rows]) * scale_value
    step_value[...] = step
    store(step_value, step_value_hbm)
    next_value[...] = weight_value[...] - 0.02 * step
    store(next_value, next_weight_value_hbm)
    loads[1].wait()
    step = update_output(factors[1, own_rows]) * scale_output
    step_output[...] = step
    store(step_output, step_output_hbm)
    next_output[...] = weight_output[...] - 0.02 * step
    store(next_output, next_weight_output_hbm)

    @pl.loop(0, model // tile)
    def _(step):
        part = pl.ds(pl.multiple_of(step * tile, tile), tile)
        copy_output[:, part] = (
            wide_output[:, part].astype(jnp.float32)
            - update_output(factors[1, part]) * (0.02 * scale_output)
        ).astype(jnp.bfloat16)
        output_copy(step).start()

    for copy in stores:
        copy.wait()
    for step in range(model // tile):
        value_copy(step).wait()
        output_copy(step).wait()


def fused_body(fs_size, tp_size, *args):
    tokens, model = args[0].shape
    cols = args[1].shape[1]
    rows, rank = args[4].shape
    ranks = args[8].shape[0]
    chips = fs_size // CORES
    depth = chips // tp_size
    f32, bf16 = jnp.float32, jnp.bfloat16
    vmem = pl.BlockSpec(memory_space=pltpu.VMEM)
    hbm = pl.BlockSpec(memory_space=pltpu.HBM)
    shape = jax.ShapeDtypeStruct
    dma = pltpu.SemaphoreType.DMA
    args = [pltpu.with_memory_space_constraint(arg, pltpu.HBM) for arg in args]
    gathered = pl.pallas_call(
        functools.partial(fused, fs_size, tp_size),
        out_shape=[
            shape((4, ranks, cols), f32),
            shape((rank, 2 * cols), bf16),
            shape((cols, rank), bf16),
            shape((2, model, rank), bf16),
            shape((2, 8, 128), f32),
            shape((model, cols), bf16),
            shape((cols, model), bf16),
        ],
        in_specs=[hbm] * 12,
        out_specs=[vmem] * 7,
        scratch_shapes=[
            pltpu.VMEM((2, tokens, model), bf16),
            pltpu.VMEM((2, tokens, cols), bf16),
            pltpu.VMEM((rows, cols), f32),
            pltpu.VMEM((cols, rows), f32),
            pltpu.VMEM((4, ranks, cols), f32),
            pltpu.VMEM((2, tokens, rank), f32),
            pltpu.VMEM((rank, tokens), bf16),
            pltpu.VMEM((chips, CORES, ranks, 2 * cols), f32),
            pltpu.VMEM((chips, ranks, 2 * cols), f32),
        ]
        + [pltpu.VMEM((depth, ranks, 2 * cols), bf16)] * 4
        + [
            pltpu.VMEM((tp_size, 2, 8, cols), f32),
            dma((12,)),
            dma((192,)),
            dma((2, fs_size)),
            dma((4, fs_size)),
            dma((fs_size,)),
            dma((chips,)),
            dma((depth,)),
            dma((depth,)),
            dma((tp_size,)),
        ],
        compiler_params=pltpu.CompilerParams(
            collective_id=0, has_side_effects=True, vmem_limit_bytes=24 * 1024 * 1024
        ),
    )(*args)

    steps = model // 256
    return pl.pallas_call(
        apply,
        out_shape=[shape((rows, cols), f32), shape((cols, rows), f32)] * 2
        + [shape((ranks, cols), f32)] * 4
        + [shape((model, cols), bf16), shape((cols, model), bf16)],
        in_specs=[vmem] * 7 + [hbm] * 2,
        out_specs=[hbm] * 10,
        scratch_shapes=[pltpu.VMEM((rows, cols), f32), pltpu.VMEM((cols, rows), f32)] * 3
        + [
            pltpu.VMEM((model, cols), bf16),
            pltpu.VMEM((cols, model), bf16),
            dma((2,)),
            dma((8,)),
            dma((steps,)),
            dma((steps,)),
        ],
        compiler_params=pltpu.CompilerParams(vmem_limit_bytes=24 * 1024 * 1024),
    )(*gathered, *args[6:8])


def solution(mesh):
    fs_size, tp_size = mesh.shape["fs"], mesh.shape["tp"]
    placed = (
        P("fs", None),
        P("fs", "tp"),
        P("fs", "tp"),
        P("fs", None),
        P("fs", None),
        P("fs", None),
        P("fs", "tp"),
        P("tp", "fs"),
        P("fs", "tp"),
        P("fs", "tp"),
        P("fs", "tp"),
        P("fs", "tp"),
    )
    chips = fs_size // CORES
    tiled = tp_size == 2 and fs_size == 16 and chips % tp_size == 0
    return jax.shard_map(
        functools.partial(fused_body, fs_size, tp_size) if tiled else body,
        mesh=mesh,
        in_specs=placed,
        out_specs=(
            P("fs", "tp"),
            P("tp", "fs"),
            P("fs", "tp"),
            P("tp", "fs"),
            P("fs", "tp"),
            P("fs", "tp"),
            P("fs", "tp"),
            P("fs", "tp"),
            P(None, "tp"),
            P("tp", None),
        ),
        check_vma=False,
    )
```

time: 130 us -> 91 us (0.70)
  the two profiles are of different devices: /device:TPU:9 before, /device:TPU:0 now
where the time goes in v1:
time: 91 us; the launch traced here: 90.8 us
  Pallas kernels  90.1 us (99%)
    pallas_call x1, Pallas kernels, fused_body(): pl.pallas_call(functools.partial(fused, fs_size, tp_size), out_shape=[sha...  83.4 us
    pallas_call x1, Pallas kernels, fused_body(): pl.pallas_call(apply, out_shape=[shape((rows, cols), f32), shape((cols, r...  6.75 us

profile of v1, /device:TPU:0, one launch (start us, length us, event | category | flops | bytes accessed | tf_op | source)
XLA Modules:
  0.0 90.8 jit_solution(14813516429007450753)
XLA Ops:
  0.6 83.4 %shard_map.195 = (f32[4,16,1024]{2,1,0:T(8,128)S(1)}, bf16[256,2048]{1,0:T(8,128)(2,1)S(1)}, bf16[1024,256]{1,0:T(8,128)(2,1)S(1)}, bf16[2,2048,256]{2,1,0:T(8,1...) custom-call(bf16[512,2048]{1,0:T(8,128)(2,1)} %input_hbm.1, ...), custom_call_target="tpu_custom_call" | custom-call | tf_op jit(solution)/shard_map/pallas_call | solution.py:629
  84.0 6.8 %shard_map.196 = (f32[128,1024]{1,0:T(8,128)}, f32[1024,128]{1,0:T(8,128)}, f32[128,1024]{1,0:T(8,128)}, f32[1024,128]{1,0:T(8,128)}, f32[16,1024]{1,0:T(8,128)}...) custom-call(f32[4,16,1024]{2,1,0:T(8,128)S(1)} %get-tuple-element.17, ...), custom_call_target="tpu_custom_call" | custom-call | tf_op jit(solution)/shard_map/pallas_call | solution.py:672

commit v2 on v1

--- a/solution.py
+++ b/solution.py
@@ -120,7 +120,7 @@
 
 class Sender:
     def __init__(self, sems):
-        self.sems, self.pending = sems, []
+        self.sems, self.pending, self.drained = sems, [], 0
 
     def send(self, source, target, recv_sem, device, when=None):
         copy = pltpu.make_async_remote_copy(
@@ -143,9 +143,11 @@
             def _():
                 action()
 
-    def drain(self):
-        for copy, when in self.pending:
+    def drain(self, count=None):
+        count = len(self.pending) if count is None else count
+        for copy, when in self.pending[self.drained : count]:
             self.guarded(copy.wait_send, when)
+        self.drained = count
 
 
 def fused(
@@ -164,10 +166,15 @@
     first_output_hbm,
     second_output_hbm,
     moments,
+    step_value,
+    step_output,
+    next_value,
+    next_output,
+    final_value,
+    final_output,
     directions,
     turned,
     factors,
-    scale_ref,
     wide_value,
     wide_output,
     stream,
@@ -175,15 +182,14 @@
     weight_value,
     weight_output,
     old,
-    projection,
     flipped,
-    terms,
-    paired,
     out_x,
     in_x,
     out_z,
     in_z,
     totals,
+    update_value,
+    update_output,
     load_sem,
     send_sem,
     factor_recv,
@@ -271,6 +277,17 @@
 
     sender = Sender(send_sem)
 
+    def projected(kind):
+        return (pl.ds(0, tokens), pl.ds(pl.multiple_of(kind * rank, rank), rank))
+
+    def term_at(to, core_at):
+        start = pl.multiple_of(tokens + (to * CORES + core_at) * ranks, ranks)
+        return update_output.at[pl.ds(start, ranks), pl.ds(0, 2 * cols)]
+
+    def paired_at(to):
+        start = pl.multiple_of(tokens + rank + to * ranks, ranks)
+        return update_output.at[pl.ds(start, ranks), pl.ds(0, 2 * cols)]
+
     def arrived(ref, recv_sem):
         pltpu.make_async_remote_copy(
             src_ref=ref,
@@ -296,12 +313,13 @@
     forward(*factor(mine, fs), over_core)
     forward(*factor(theirs, fs), over_core)
 
-    half_rows, half_cols = rows // 2, cols // 2
+    direct = (1,)
+    lead, half_cols = rows // 2, cols // 2
 
     def piece(part, origin):
         start = pl.multiple_of(origin * rows, rows)
         if part < 2:
-            ref = wide_value.at[pl.ds(start + part * half_rows, half_rows)]
+            ref = wide_value.at[pl.ds(start + part * lead, rows - lead if part else lead)]
         else:
             ref = wide_output.at[pl.ds((part - 2) * half_cols, half_cols), pl.ds(start, rows)]
         return ref, weight_recv.at[part, origin]
@@ -309,32 +327,50 @@
     def piece_z(part, origin):
         forward(*piece(part, origin), along_z(beside))
         forward(*piece(part, origin), along_z(mirror), middle)
-        forward(*piece(part, origin), along_z(across))
-
-    beyond = along_z(jnp.clip(last * (z - 1), 0, last))
-
-    def piece_arrives_z(part, x_at, cross):
-        for z_at in others:
-            ref, sem = piece(part, index(z_at, x_at, core))
+        if part in direct:
+            forward(*piece(part, origin), along_z(across))
+
+    def piece_from_z(part, z_at, x_at, onward, when=None):
+        ref, sem = piece(part, index(z_at, x_at, core))
+        sender.guarded(lambda: arrived(ref, sem), when)
+        if onward is not None:
+            forward(ref, sem, along_z(onward), middle)
+        forward(ref, sem, over_core, when)
+
+    def near(part, x_at):
+        relayed = part not in direct
+        piece_from_z(part, beside, x_at, mirror if relayed else None)
+        piece_from_z(part, mirror, x_at, beside if relayed else None, middle)
+
+    def second(part, x_at):
+        piece_from_z(part, across, x_at, beside)
+
+    def third(part, x_at):
+        piece_from_z(part, mirror, x_at, None, jnp.logical_not(middle))
+
+    def cross(part, *z_ats):
+        for z_at in z_ats:
+            forward(*piece(part, index(z_at, x, core)), over_x)
+
+    def to_core(part, *z_ats):
+        for z_at in z_ats:
+            forward(*piece(part, index(z_at, x, core)), over_core)
+
+    def from_x(part, *z_ats):
+        for z_at in z_ats:
+            ref, sem = piece(part, index(z_at, 1 - x, core))
             arrived(ref, sem)
-            if z_at is across:
-                forward(ref, sem, beyond, middle)
-            if cross:
-                forward(ref, sem, over_x)
             forward(ref, sem, over_core)
-
-    def piece_arrives_x(part, z_at):
-        ref, sem = piece(part, index(z_at, 1 - x, core))
-        arrived(ref, sem)
-        forward(ref, sem, over_core)
 
     loads[2].wait()
     loads[3].wait()
     own_rows = pl.ds(pl.multiple_of(fs * rows, rows), rows)
     wide_value[own_rows, :] = weight_value[...].astype(jnp.bfloat16)
     wide_output[:, own_rows] = weight_output[...].astype(jnp.bfloat16)
+    cross(0, z)
     piece_z(1, fs)
     piece_z(2, fs)
+    piece_z(3, fs)
 
     for z_at in others:
         ref, sem = factor(mine, index(z_at, x, core))
@@ -342,8 +378,8 @@
         forward(ref, sem, over_x)
         forward(ref, sem, over_y)
         forward(ref, sem, over_core)
-    for part in range(4):
-        forward(*piece(part, fs), over_x)
+    for part in (1, 2, 3):
+        cross(part, z)
     ref, sem = factor(theirs, index(z, 1 - x, core))
     arrived(ref, sem)
     forward(ref, sem, over_core)
@@ -362,7 +398,8 @@
         product = jnp.dot(
             stream[kind, :, part], factors[kind, part], preferred_element_type=jnp.float32
         )
-        projection[kind] = product if first else projection[kind] + product
+        at = projected(kind)
+        update_output[at] = product if first else update_output[at] + product
 
     def from_y(z_at, x_at):
         ref, sem = factor(theirs, index(z_at, x_at, core))
@@ -380,38 +417,44 @@
     for z_at in others:
         from_y(z_at, 1 - x)
     for part in range(4):
-        forward(*piece(part, fs), over_core)
+        to_core(part, z)
+    near(1, x)
     for z_at in others:
         project(theirs, z_at, x)
     for z_at in (z,) + others:
         project(theirs, z_at, 1 - x)
 
+    second(1, x)
+    near(2, x)
+    cross(1, beside)
     width_tile = 256
     for kind in range(2):
-        flipped[...] = projection[kind].T.astype(jnp.bfloat16)
+        flipped[...] = update_output[projected(kind)].T.astype(jnp.bfloat16)
 
         @pl.loop(0, cols // width_tile)
         def _(step, kind=kind):
             tile = pl.ds(pl.multiple_of(step * width_tile, width_tile), width_tile)
             term = jnp.dot(flipped[...], cotan[kind, :, tile], preferred_element_type=jnp.float32)
             target = pl.ds(pl.multiple_of(kind * cols + step * width_tile, width_tile), width_tile)
-            terms[:, :, :, target] = term.reshape(chips, CORES, ranks, width_tile)
+            update_output[tokens : tokens + rank, target] = term
 
     far = others + (z,)
     for x_at in (1 - x, x):
         for z_at in far:
             to = z_at * width + x_at
-            sender.send(terms.at[to, 1 - core], paired.at[to], pair_recv.at[to], over_core)
+            sender.send(term_at(to, 1 - core), paired_at(to), pair_recv.at[to], over_core)
 
     def pair_sum(z_at, x_at):
         at = z_at * width + x_at
-        arrived(paired.at[at], pair_recv.at[at])
-        return terms[at, core] + paired[at]
+        arrived(paired_at(at), pair_recv.at[at])
+        return term_at(at, core)[...] + paired_at(at)[...]
 
     for z_at in far:
         out_x[z_at] = pair_sum(z_at, 1 - x).astype(jnp.bfloat16)
         sender.send(out_x.at[z_at], in_x.at[z_at], x_recv.at[z_at], over_x)
-    piece_arrives_z(1, x, True)
+    cross(1, across)
+    near(3, x)
+    from_x(0, z)
 
     def column_sum(z_at):
         total = pair_sum(z_at, x)
@@ -421,8 +464,12 @@
     for z_at in others:
         out_z[z_at] = column_sum(z_at).astype(jnp.bfloat16)
         sender.send(out_z.at[z_at], in_z.at[z], z_recv.at[z], along_z(z_at))
-    piece_z(3, fs)
+    early = len(sender.pending)
     low = column_sum(z)
+    second(2, x)
+    piece_z(0, fs)
+    for part in (1, 2, 3):
+        from_x(part, z)
     for z_at in others:
         arrived(in_z.at[z_at], z_recv.at[z_at])
         low = low + in_z[z_at].astype(jnp.float32)
@@ -444,15 +491,20 @@
         forward(*direction(fs), along_z(z_at))
     forward(*direction(fs), over_x)
     forward(*direction(fs), over_core)
+    cross(2, beside)
+    second(3, x)
+    cross(3, beside)
+    piece_z(0, index(z, 1 - x, core))
     for z_at in others:
         ref, sem = direction(index(z_at, x, core))
         arrived(ref, sem)
         forward(ref, sem, over_x)
         forward(ref, sem, over_core)
-    piece_arrives_x(0, z)
-    piece_z(0, fs)
-    piece_z(0, index(z, 1 - x, core))
-    piece_arrives_z(2, x, True)
+    cross(2, across)
+    third(1, x)
+    cross(1, mirror)
+    near(0, x)
+    from_x(1, beside, across)
     for z_at in (z,) + others:
         ref, sem = direction(index(z_at, 1 - x, core))
         arrived(ref, sem)
@@ -460,157 +512,106 @@
     for z_at in (z,) + others:
         for x_at in (x, 1 - x):
             arrived(*direction(index(z_at, x_at, 1 - core)))
-
-    tile = 256
-    for kind in range(2):
+    def total_of(kind):
         totals[tp, kind] = jnp.zeros((8, cols), jnp.float32)
 
-        @pl.loop(0, model // tile)
-        def _(step, kind=kind):
-            update = jnp.dot(
-                factors[kind, pl.ds(pl.multiple_of(step * tile, tile), tile)],
-                directions[:, kind * cols : (kind + 1) * cols],
-                preferred_element_type=jnp.float32,
-            )
-            totals[tp, kind] += jnp.sum((update * update).reshape(tile // 8, 8, cols), axis=0)
-
+        @pl.loop(0, chips)
+        def _(step):
+            part = pl.ds(pl.multiple_of(step * span, span), span)
+            if kind == 0:
+                update = jnp.dot(
+                    factors[0, part], directions[:, :cols], preferred_element_type=jnp.float32
+                )
+                update_value[part] = update
+            else:
+                update = lax.dot_general(
+                    turned[...],
+                    factors[1, part],
+                    (((1,), (1,)), ((), ())),
+                    preferred_element_type=jnp.float32,
+                )
+                update_output[:, part] = update
+            square = update * update
+            lanes = square.shape[1]
+            totals[tp, kind, :, :lanes] += jnp.sum(square.reshape(-1, 8, lanes), axis=0)
+
+    cross(3, across)
+    third(2, x)
+    cross(2, mirror)
+    near(0, 1 - x)
+    sender.drain(early)
+    total_of(0)
+    second(0, x)
+    third(3, x)
+    cross(3, mirror)
+    turned[...] = directions[:, cols:].astype(jnp.float32).T.astype(jnp.bfloat16)
+    total_of(1)
     sender.send(totals.at[tp], totals.at[tp], total_recv.at[tp], over_y)
-    turned[...] = directions[:, cols:].astype(jnp.float32).T.astype(jnp.bfloat16)
-
-    piece_arrives_z(3, x, True)
-    for z_at in (z,) + others:
-        piece_arrives_x(1, z_at)
-    piece_arrives_z(0, x, False)
-    piece_arrives_z(0, 1 - x, False)
+    second(0, 1 - x)
+    from_x(1, mirror)
+    from_x(2, beside, across)
+    from_x(3, beside)
     arrived(totals.at[1 - tp], total_recv.at[1 - tp])
     entries = model * cols * tp_size
-    for kind in range(2):
-        total = jnp.sum(totals[0, kind] + totals[1, kind], keepdims=True)
-        scale = lax.rsqrt(total / entries + 1e-06)
-        scale_ref[kind] = jnp.broadcast_to(scale, scale_ref.shape[1:])
-    for part in (2, 3):
-        for z_at in (z,) + others:
-            piece_arrives_x(part, z_at)
-    for part in range(4):
-        for z_at in (z,) + others:
-            for x_at in (x, 1 - x):
-                arrived(*piece(part, index(z_at, x_at, 1 - core)))
+    scales = [
+        lax.rsqrt(jnp.sum(totals[0, kind] + totals[1, kind], keepdims=True) / entries + 1e-06)
+        for kind in range(2)
+    ]
+    def finals(kind, z_at, x_at):
+        for part in (2 * kind, 2 * kind + 1):
+            arrived(*piece(part, index(z_at, x_at, 1 - core)))
+        part = pl.ds(pl.multiple_of((z_at * width + x_at) * span, span), span)
+        scale = 0.02 * scales[kind]
+        if kind == 0:
+            final_value[part] = (
+                wide_value[part].astype(jnp.float32) - update_value[part] * scale
+            ).astype(jnp.bfloat16)
+        else:
+            final_output[:, part] = (
+                wide_output[:, part].astype(jnp.float32) - update_output[:, part] * scale
+            ).astype(jnp.bfloat16)
+
+    step = update_value[own_rows] * scales[0]
+    step_value[...] = step
+    next_value[...] = weight_value[...] - 0.02 * step
+    step = update_output[:, own_rows] * scales[1]
+    step_output[...] = step
+    next_output[...] = weight_output[...] - 0.02 * step
+    finals(0, z, x)
+    finals(1, z, x)
+    finals(1, beside, x)
+    from_x(3, across)
+    third(0, x)
+    finals(0, beside, x)
+    finals(0, across, x)
+    finals(1, across, x)
+    from_x(2, mirror)
+    finals(1, z, 1 - x)
+    third(0, 1 - x)
+    for z_at in (z, beside, across):
+        finals(0, z_at, 1 - x)
+    finals(1, beside, 1 - x)
+    from_x(3, mirror)
+    finals(0, mirror, x)
+    finals(1, mirror, x)
+    finals(0, mirror, 1 - x)
+    finals(1, across, 1 - x)
+    finals(1, mirror, 1 - x)
     sender.drain()
 
 
-def apply(
-    moments,
-    directions,
-    turned,
-    factors,
-    scale_ref,
-    wide_value,
-    wide_output,
-    weight_value_hbm,
-    weight_output_hbm,
-    step_value_hbm,
-    step_output_hbm,
-    next_weight_value_hbm,
-    next_weight_output_hbm,
-    next_first_value_hbm,
-    next_second_value_hbm,
-    next_first_output_hbm,
-    next_second_output_hbm,
-    copy_value_hbm,
-    copy_output_hbm,
-    weight_value,
-    weight_output,
-    step_value,
-    step_output,
-    next_value,
-    next_output,
-    copy_value,
-    copy_output,
-    load_sem,
-    store_sem,
-    value_sem,
-    output_sem,
-):
-    rows, cols = weight_value_hbm.shape
-    model = factors.shape[1]
-    fs = lax.axis_index("fs")
-    scale_value, scale_output = scale_ref[0, :1, :1], scale_ref[1, :1, :1]
-    transposed = (((1,), (1,)), ((), ()))
-    loads = [
-        pltpu.make_async_copy(weight_value_hbm, weight_value, load_sem.at[0]),
-        pltpu.make_async_copy(weight_output_hbm, weight_output, load_sem.at[1]),
+def write(count, *refs):
+    sems = refs[-1]
+    copies = [
+        pltpu.make_async_copy(source, target, sems.at[slot])
+        for slot, (source, target) in enumerate(
+            zip(refs[1:count] + tuple(refs[0].at[k] for k in range(4)), refs[count:-1])
+        )
     ]
-    for load in loads:
-        load.start()
-    stores = []
-
-    def store(source, target):
-        copy = pltpu.make_async_copy(source, target, store_sem.at[len(stores)])
+    for copy in copies:
         copy.start()
-        stores.append(copy)
-
-    store(moments.at[0], next_first_value_hbm)
-    store(moments.at[1], next_second_value_hbm)
-    store(moments.at[2], next_first_output_hbm)
-    store(moments.at[3], next_second_output_hbm)
-
-    def update_value(factor):
-        return jnp.dot(factor, directions[:, :cols], preferred_element_type=jnp.float32)
-
-    def update_output(factor):
-        return lax.dot_general(turned[...], factor, transposed, preferred_element_type=jnp.float32)
-
-    tile = 256
-
-    def value_copy(step):
-        part = pl.ds(pl.multiple_of(step * tile, tile), tile)
-        return pltpu.make_async_copy(
-            copy_value.at[part], copy_value_hbm.at[part], value_sem.at[step]
-        )
-
-    def output_copy(step):
-        part = pl.ds(pl.multiple_of(step * tile, tile), tile)
-        return pltpu.make_async_copy(
-            copy_output.at[:, part], copy_output_hbm.at[:, part], output_sem.at[step]
-        )
-
-    @pl.loop(0, model // tile)
-    def _(step):
-        part = pl.ds(pl.multiple_of(step * tile, tile), tile)
-        copy_value[part] = (
-            wide_value[part].astype(jnp.float32)
-            - update_value(factors[0, part]) * (0.02 * scale_value)
-        ).astype(jnp.bfloat16)
-        value_copy(step).start()
-
-    own_rows = pl.ds(pl.multiple_of(fs * rows, rows), rows)
-    loads[0].wait()
-    step = update_value(factors[0, own_rows]) * scale_value
-    step_value[...] = step
-    store(step_value, step_value_hbm)
-    next_value[...] = weight_value[...] - 0.02 * step
-    store(next_value, next_weight_value_hbm)
-    loads[1].wait()
-    step = update_output(factors[1, own_rows]) * scale_output
-    step_output[...] = step
-    store(step_output, step_output_hbm)
-    next_output[...] = weight_output[...] - 0.02 * step
-    store(next_output, next_weight_output_hbm)
-
-    @pl.loop(0, model // tile)
-    def _(step):
-        part = pl.ds(pl.multiple_of(step * tile, tile), tile)
-        copy_output[:, part] = (
-            wide_output[:, part].astype(jnp.float32)
-            - update_output(factors[1, part]) * (0.02 * scale_output)
-        ).astype(jnp.bfloat16)
-        output_copy(step).start()
-
-    for copy in stores:
+    for copy in copies:
         copy.wait()
-    for step in range(model // tile):
-        value_copy(step).wait()
-        output_copy(step).wait()
 
 
 def fused_body(fs_size, tp_size, *args):
@@ -626,35 +627,33 @@
     shape = jax.ShapeDtypeStruct
     dma = pltpu.SemaphoreType.DMA
     args = [pltpu.with_memory_space_constraint(arg, pltpu.HBM) for arg in args]
-    gathered = pl.pallas_call(
+    own = [shape((rows, cols), f32), shape((cols, rows), f32)] * 2
+    copies = [shape((model, cols), bf16), shape((cols, model), bf16)]
+    results = pl.pallas_call(
         functools.partial(fused, fs_size, tp_size),
-        out_shape=[
-            shape((4, ranks, cols), f32),
-            shape((rank, 2 * cols), bf16),
-            shape((cols, rank), bf16),
-            shape((2, model, rank), bf16),
-            shape((2, 8, 128), f32),
-            shape((model, cols), bf16),
-            shape((cols, model), bf16),
-        ],
+        out_shape=[shape((4, ranks, cols), f32)] + own + copies,
         in_specs=[hbm] * 12,
         out_specs=[vmem] * 7,
         scratch_shapes=[
+            pltpu.VMEM((rank, 2 * cols), bf16),
+            pltpu.VMEM((cols, rank), bf16),
+            pltpu.VMEM((2, model, rank), bf16),
+            pltpu.VMEM((model, cols), bf16),
+            pltpu.VMEM((cols, model), bf16),
             pltpu.VMEM((2, tokens, model), bf16),
             pltpu.VMEM((2, tokens, cols), bf16),
             pltpu.VMEM((rows, cols), f32),
             pltpu.VMEM((cols, rows), f32),
             pltpu.VMEM((4, ranks, cols), f32),
-            pltpu.VMEM((2, tokens, rank), f32),
             pltpu.VMEM((rank, tokens), bf16),
-            pltpu.VMEM((chips, CORES, ranks, 2 * cols), f32),
-            pltpu.VMEM((chips, ranks, 2 * cols), f32),
         ]
         + [pltpu.VMEM((depth, ranks, 2 * cols), bf16)] * 4
         + [
             pltpu.VMEM((tp_size, 2, 8, cols), f32),
+            pltpu.VMEM((model, cols), f32),
+            pltpu.VMEM((cols, model), f32),
             dma((12,)),
-            dma((192,)),
+            dma((136,)),
             dma((2, fs_size)),
             dma((4, fs_size)),
             dma((fs_size,)),
@@ -664,29 +663,19 @@
             dma((tp_size,)),
         ],
         compiler_params=pltpu.CompilerParams(
-            collective_id=0, has_side_effects=True, vmem_limit_bytes=24 * 1024 * 1024
+            collective_id=0, has_side_effects=True, vmem_limit_bytes=40 * 1024 * 1024
         ),
     )(*args)
 
-    steps = model // 256
-    return pl.pallas_call(
-        apply,
-        out_shape=[shape((rows, cols), f32), shape((cols, rows), f32)] * 2
-        + [shape((ranks, cols), f32)] * 4
-        + [shape((model, cols), bf16), shape((cols, model), bf16)],
-        in_specs=[vmem] * 7 + [hbm] * 2,
+    written = pl.pallas_call(
+        functools.partial(write, len(results)),
+        out_shape=own + copies + [shape((ranks, cols), f32)] * 4,
+        in_specs=[vmem] * len(results),
         out_specs=[hbm] * 10,
-        scratch_shapes=[pltpu.VMEM((rows, cols), f32), pltpu.VMEM((cols, rows), f32)] * 3
-        + [
-            pltpu.VMEM((model, cols), bf16),
-            pltpu.VMEM((cols, model), bf16),
-            dma((2,)),
-            dma((8,)),
-            dma((steps,)),
-            dma((steps,)),
-        ],
-        compiler_params=pltpu.CompilerParams(vmem_limit_bytes=24 * 1024 * 1024),
-    )(*gathered, *args[6:8])
+        scratch_shapes=[dma((10,))],
+        compiler_params=pltpu.CompilerParams(vmem_limit_bytes=1024 * 1024),
+    )(*results)
+    return written[:4] + written[6:] + written[4:6]
 
 
 def solution(mesh):

time: 91 us -> 75.3 us (0.83)
  Pallas kernels: 90.1 us -> 74.4 us
    pallas_call x1, Pallas kernels: 83.4 us -> 70.3 us  [fused_body(): pl.pallas_call(functools.partial(fused, fs_size, tp_size), out_shape=[sha...]
    pallas_call x1, Pallas kernels: 6.75 us -> 4.19 us  [fused_body(): pl.pallas_call(functools.partial(write, len(results)), out_shape=own + co...]
where the time goes in v2:
time: 75.3 us; the launch traced here: 75.1 us
  Pallas kernels  74.4 us (99%)
    pallas_call x1, Pallas kernels, fused_body(): pl.pallas_call(functools.partial(fused, fs_size, tp_size), out_shape=[sha...  70.3 us
    pallas_call x1, Pallas kernels, fused_body(): pl.pallas_call(functools.partial(write, len(results)), out_shape=own + co...  4.19 us

profile of v2, /device:TPU:0, one launch (start us, length us, event | category | flops | bytes accessed | tf_op | source)
XLA Modules:
  0.0 75.1 jit_solution(7473640120632845000)
XLA Ops:
  0.6 70.3 %shard_map.195 = (f32[4,16,1024]{2,1,0:T(8,128)S(1)}, f32[128,1024]{1,0:T(8,128)S(1)}, f32[1024,128]{1,0:T(8,128)S(1)}, f32[128,1024]{1,0:T(8,128)S(1)}, f32[102...) custom-call(bf16[512,2048]{1,0:T(8,128)(2,1)} %input_hbm.1, ...), custom_call_target="tpu_custom_call" | custom-call | tf_op jit(solution)/shard_map/pallas_call | solution.py:632
  70.9 4.2 %shard_map.196 = (f32[128,1024]{1,0:T(8,128)}, f32[1024,128]{1,0:T(8,128)}, f32[128,1024]{1,0:T(8,128)}, f32[1024,128]{1,0:T(8,128)}, bf16[2048,1024]{1,0:T(8,12...) custom-call(f32[4,16,1024]{2,1,0:T(8,128)S(1)} %get-tuple-element.27, ...), custom_call_target="tpu_custom_call" | custom-call | tf_op jit(solution)/shard_map/pallas_call | solution.py:670

commit v3 on v2

--- a/solution.py
+++ b/solution.py
@@ -123,10 +123,12 @@
         self.sems, self.pending, self.drained = sems, [], 0
 
     def send(self, source, target, recv_sem, device, when=None):
+        slots = self.sems.shape[0]
+        self.drain(len(self.pending) + 1 - slots)
         copy = pltpu.make_async_remote_copy(
             src_ref=source,
             dst_ref=target,
-            send_sem=self.sems.at[len(self.pending)],
+            send_sem=self.sems.at[len(self.pending) % slots],
             recv_sem=recv_sem,
             device_id=device,
             device_id_type=MESH,
@@ -144,7 +146,7 @@
                 action()
 
     def drain(self, count=None):
-        count = len(self.pending) if count is None else count
+        count = max(len(self.pending) if count is None else count, self.drained)
         for copy, when in self.pending[self.drained : count]:
             self.guarded(copy.wait_send, when)
         self.drained = count
@@ -187,6 +189,7 @@
     in_x,
     out_z,
     in_z,
+    squares,
     totals,
     update_value,
     update_output,
@@ -194,7 +197,9 @@
     send_sem,
     factor_recv,
     weight_recv,
+    core_recv,
     direction_recv,
+    join_recv,
     pair_recv,
     x_recv,
     z_recv,
@@ -223,12 +228,17 @@
     over_x = {"fs": index(z, 1 - x, core)}
     over_core = {"fs": index(z, x, 1 - core)}
     over_y = {"tp": 1 - tp}
+    diagonal = {**over_core, **over_y}
     beside = z + 1 - 2 * lax.rem(z, 2)
     mirror = last - z
     across = lax.rem(z + depth // 2, depth)
     others = (beside, mirror, across)
     middle = jnp.logical_and(z > 0, z < last)
 
+    barrier = pltpu.get_barrier_semaphore()
+    peers = [along_z(z_at) for z_at in others] + [over_x, over_core, over_y, diagonal]
+    for peer in peers:
+        pl.semaphore_signal(barrier, inc=1, device_id=peer, device_id_type=MESH)
     def block(ref, origin, size):
         return ref.at[pl.ds(pl.multiple_of(origin * size, size), size)]
 
@@ -267,10 +277,6 @@
     for load in loads:
         load.start()
 
-    barrier = pltpu.get_barrier_semaphore()
-    peers = [along_z(z_at) for z_at in others] + [over_x, over_core, over_y]
-    for peer in peers:
-        pl.semaphore_signal(barrier, inc=1, device_id=peer, device_id_type=MESH)
     loads[0].wait()
     loads[1].wait()
     pl.semaphore_wait(barrier, len(peers))
@@ -314,7 +320,7 @@
     forward(*factor(theirs, fs), over_core)
 
     direct = (1,)
-    lead, half_cols = rows // 2, cols // 2
+    lead, half_cols = rows * 3 // 8, cols // 2
 
     def piece(part, origin):
         start = pl.multiple_of(origin * rows, rows)
@@ -322,7 +328,11 @@
             ref = wide_value.at[pl.ds(start + part * lead, rows - lead if part else lead)]
         else:
             ref = wide_output.at[pl.ds((part - 2) * half_cols, half_cols), pl.ds(start, rows)]
-        return ref, weight_recv.at[part, origin]
+        return ref, weight_recv.at[part, origin // CORES]
+
+    def piece_to_core(part, origin, when=None):
+        ref, _ = piece(part, origin)
+        forward(ref, core_recv.at[part // 2, origin // CORES], over_core, when)
 
     def piece_z(part, origin):
         forward(*piece(part, origin), along_z(beside))
@@ -335,7 +345,7 @@
         sender.guarded(lambda: arrived(ref, sem), when)
         if onward is not None:
             forward(ref, sem, along_z(onward), middle)
-        forward(ref, sem, over_core, when)
+        piece_to_core(part, index(z_at, x_at, core), when)
 
     def near(part, x_at):
         relayed = part not in direct
@@ -354,13 +364,12 @@
 
     def to_core(part, *z_ats):
         for z_at in z_ats:
-            forward(*piece(part, index(z_at, x, core)), over_core)
+            piece_to_core(part, index(z_at, x, core))
 
     def from_x(part, *z_ats):
         for z_at in z_ats:
-            ref, sem = piece(part, index(z_at, 1 - x, core))
-            arrived(ref, sem)
-            forward(ref, sem, over_core)
+            arrived(*piece(part, index(z_at, 1 - x, core)))
+            piece_to_core(part, index(z_at, 1 - x, core))
 
     loads[2].wait()
     loads[3].wait()
@@ -425,7 +434,6 @@
         project(theirs, z_at, 1 - x)
 
     second(1, x)
-    near(2, x)
     cross(1, beside)
     width_tile = 256
     for kind in range(2):
@@ -452,6 +460,7 @@
     for z_at in far:
         out_x[z_at] = pair_sum(z_at, 1 - x).astype(jnp.bfloat16)
         sender.send(out_x.at[z_at], in_x.at[z_at], x_recv.at[z_at], over_x)
+    near(2, x)
     cross(1, across)
     near(3, x)
     from_x(0, z)
@@ -466,8 +475,8 @@
         sender.send(out_z.at[z_at], in_z.at[z], z_recv.at[z], along_z(z_at))
     early = len(sender.pending)
     low = column_sum(z)
+    cross(2, beside)
     second(2, x)
-    piece_z(0, fs)
     for part in (1, 2, 3):
         from_x(part, z)
     for z_at in others:
@@ -485,39 +494,44 @@
         ).astype(jnp.bfloat16)
 
     def direction(origin):
-        return block(directions, origin, ranks), direction_recv.at[origin]
+        return block(directions, origin, ranks), direction_recv.at[origin // CORES]
 
     for z_at in others:
         forward(*direction(fs), along_z(z_at))
     forward(*direction(fs), over_x)
-    forward(*direction(fs), over_core)
-    cross(2, beside)
+    forward(direction(fs)[0], join_recv.at[0], over_core)
+    cross(3, beside)
+    cross(2, across)
+    piece_z(0, fs)
     second(3, x)
-    cross(3, beside)
     piece_z(0, index(z, 1 - x, core))
     for z_at in others:
         ref, sem = direction(index(z_at, x, core))
         arrived(ref, sem)
         forward(ref, sem, over_x)
-        forward(ref, sem, over_core)
-    cross(2, across)
+        forward(ref, join_recv.at[0], over_core)
     third(1, x)
     cross(1, mirror)
-    near(0, x)
     from_x(1, beside, across)
     for z_at in (z,) + others:
         ref, sem = direction(index(z_at, 1 - x, core))
         arrived(ref, sem)
-        forward(ref, sem, over_core)
-    for z_at in (z,) + others:
-        for x_at in (x, 1 - x):
-            arrived(*direction(index(z_at, x_at, 1 - core)))
-    def total_of(kind):
-        totals[tp, kind] = jnp.zeros((8, cols), jnp.float32)
-
-        @pl.loop(0, chips)
+        forward(ref, join_recv.at[0], over_core)
+    near(0, x)
+    cross(3, across)
+    third(2, x)
+    cross(2, mirror)
+    arrived(directions.at[pl.ds(0, chips * ranks)], join_recv.at[0])
+    half = chips // CORES
+    me = tp * CORES + core
+
+    def updates(kind, side, counted):
+        if counted:
+            squares[kind] = jnp.zeros((8, cols), jnp.float32)
+
+        @pl.loop(0, half)
         def _(step):
-            part = pl.ds(pl.multiple_of(step * span, span), span)
+            part = pl.ds(pl.multiple_of((side * half + step) * span, span), span)
             if kind == 0:
                 update = jnp.dot(
                     factors[0, part], directions[:, :cols], preferred_element_type=jnp.float32
@@ -531,35 +545,45 @@
                     preferred_element_type=jnp.float32,
                 )
                 update_output[:, part] = update
-            square = update * update
-            lanes = square.shape[1]
-            totals[tp, kind, :, :lanes] += jnp.sum(square.reshape(-1, 8, lanes), axis=0)
-
-    cross(3, across)
-    third(2, x)
-    cross(2, mirror)
+            if counted:
+                square = update * update
+                lanes = square.shape[1]
+                squares[kind, :, :lanes] += jnp.sum(square.reshape(-1, 8, lanes), axis=0)
+
+        if counted:
+            folded = squares[kind, :, :128]
+            for lane in range(128, cols, 128):
+                folded = folded + squares[kind, :, lane : lane + 128]
+            totals[me, kind] = folded
+
+    sender.drain(early)
+    updates(0, core, True)
     near(0, 1 - x)
-    sender.drain(early)
-    total_of(0)
+    turned[...] = directions[:, cols:].astype(jnp.float32).T.astype(jnp.bfloat16)
     second(0, x)
     third(3, x)
     cross(3, mirror)
-    turned[...] = directions[:, cols:].astype(jnp.float32).T.astype(jnp.bfloat16)
-    total_of(1)
-    sender.send(totals.at[tp], totals.at[tp], total_recv.at[tp], over_y)
+    updates(1, core, True)
+    for device in (over_y, over_core, diagonal):
+        sender.send(totals.at[me], totals.at[me], total_recv.at[me], device)
     second(0, 1 - x)
+    updates(0, 1 - core, False)
+    updates(1, 1 - core, False)
     from_x(1, mirror)
     from_x(2, beside, across)
     from_x(3, beside)
-    arrived(totals.at[1 - tp], total_recv.at[1 - tp])
+    for tp_at, core_at in ((tp, 1 - core), (1 - tp, core), (1 - tp, 1 - core)):
+        slot = tp_at * CORES + core_at
+        arrived(totals.at[slot], total_recv.at[slot])
     entries = model * cols * tp_size
     scales = [
-        lax.rsqrt(jnp.sum(totals[0, kind] + totals[1, kind], keepdims=True) / entries + 1e-06)
+        lax.rsqrt(jnp.sum(jnp.sum(totals[:, kind], axis=0), keepdims=True) / entries + 1e-06)
         for kind in range(2)
     ]
     def finals(kind, z_at, x_at):
-        for part in (2 * kind, 2 * kind + 1):
-            arrived(*piece(part, index(z_at, x_at, 1 - core)))
+        at = z_at * width + x_at
+        sent = pl.ds(pl.multiple_of((at * CORES + 1 - core) * rows, rows), rows)
+        arrived((wide_output.at[:, sent] if kind else wide_value.at[sent]), core_recv.at[kind, at])
         part = pl.ds(pl.multiple_of((z_at * width + x_at) * span, span), span)
         scale = 0.02 * scales[kind]
         if kind == 0:
@@ -602,11 +626,11 @@
 
 def write(count, *refs):
     sems = refs[-1]
+    sources = refs[5:count] + refs[1:5] + tuple(refs[0].at[k] for k in range(4))
+    targets = refs[count + 4 : count + 6] + refs[count : count + 4] + refs[count + 6 : -1]
     copies = [
         pltpu.make_async_copy(source, target, sems.at[slot])
-        for slot, (source, target) in enumerate(
-            zip(refs[1:count] + tuple(refs[0].at[k] for k in range(4)), refs[count:-1])
-        )
+        for slot, (source, target) in enumerate(zip(sources, targets))
     ]
     for copy in copies:
         copy.start()
@@ -649,18 +673,21 @@
         ]
         + [pltpu.VMEM((depth, ranks, 2 * cols), bf16)] * 4
         + [
-            pltpu.VMEM((tp_size, 2, 8, cols), f32),
+            pltpu.VMEM((2, 8, cols), f32),
+            pltpu.VMEM((tp_size * CORES, 2, 8, 128), f32),
             pltpu.VMEM((model, cols), f32),
             pltpu.VMEM((cols, model), f32),
             dma((12,)),
-            dma((136,)),
+            dma((40,)),
             dma((2, fs_size)),
-            dma((4, fs_size)),
-            dma((fs_size,)),
+            dma((4, chips)),
+            dma((2, chips)),
+            dma((chips,)),
+            dma((1,)),
             dma((chips,)),
             dma((depth,)),
             dma((depth,)),
-            dma((tp_size,)),
+            dma((tp_size * CORES,)),
         ],
         compiler_params=pltpu.CompilerParams(
             collective_id=0, has_side_effects=True, vmem_limit_bytes=40 * 1024 * 1024

time: 75.3 us -> 71.4 us (0.948)
  Pallas kernels: 74.4 us -> 70.5 us
    pallas_call x1, Pallas kernels: 70.3 us -> 66.4 us  [fused_body(): pl.pallas_call(functools.partial(fused, fs_size, tp_size), out_shape=[sha...]
where the time goes in v3:
time: 71.4 us; the launch traced here: 71.1 us
  Pallas kernels  70.5 us (99%)
    pallas_call x1, Pallas kernels, fused_body(): pl.pallas_call(functools.partial(fused, fs_size, tp_size), out_shape=[sha...  66.4 us
    pallas_call x1, Pallas kernels, fused_body(): pl.pallas_call(functools.partial(write, len(results)), out_shape=own + co...  4.06 us

profile of v3, /device:TPU:0, one launch (start us, length us, event | category | flops | bytes accessed | tf_op | source)
XLA Modules:
  0.0 71.1 jit_solution(13606081833453275754)
XLA Ops:
  0.6 66.4 %shard_map.195 = (f32[4,16,1024]{2,1,0:T(8,128)S(1)}, f32[128,1024]{1,0:T(8,128)S(1)}, f32[1024,128]{1,0:T(8,128)S(1)}, f32[128,1024]{1,0:T(8,128)S(1)}, f32[102...) custom-call(bf16[512,2048]{1,0:T(8,128)(2,1)} %input_hbm.1, ...), custom_call_target="tpu_custom_call" | custom-call | tf_op jit(solution)/shard_map/pallas_call | solution.py:656
  67.1 4.1 %shard_map.196 = (f32[128,1024]{1,0:T(8,128)}, f32[1024,128]{1,0:T(8,128)}, f32[128,1024]{1,0:T(8,128)}, f32[1024,128]{1,0:T(8,128)}, bf16[2048,1024]{1,0:T(8,12...) custom-call(f32[4,16,1024]{2,1,0:T(8,128)S(1)} %get-tuple-element.27, ...), custom_call_target="tpu_custom_call" | custom-call | tf_op jit(solution)/shard_map/pallas_call | solution.py:697

commit v4 on v3

--- a/solution.py
+++ b/solution.py
@@ -425,9 +425,22 @@
         project(mine, z_at, 1 - x)
     for z_at in others:
         from_y(z_at, 1 - x)
+    width_tile = 256
+
+    def terms_of(kind):
+        flipped[...] = update_output[projected(kind)].T.astype(jnp.bfloat16)
+
+        @pl.loop(0, cols // width_tile)
+        def _(step):
+            tile = pl.ds(pl.multiple_of(step * width_tile, width_tile), width_tile)
+            term = jnp.dot(flipped[...], cotan[kind, :, tile], preferred_element_type=jnp.float32)
+            start = pl.multiple_of(kind * cols + step * width_tile, width_tile)
+            update_output[tokens : tokens + rank, pl.ds(start, width_tile)] = term
+
     for part in range(4):
         to_core(part, z)
     near(1, x)
+    terms_of(mine)
     for z_at in others:
         project(theirs, z_at, x)
     for z_at in (z,) + others:
@@ -435,16 +448,7 @@
 
     second(1, x)
     cross(1, beside)
-    width_tile = 256
-    for kind in range(2):
-        flipped[...] = update_output[projected(kind)].T.astype(jnp.bfloat16)
-
-        @pl.loop(0, cols // width_tile)
-        def _(step, kind=kind):
-            tile = pl.ds(pl.multiple_of(step * width_tile, width_tile), width_tile)
-            term = jnp.dot(flipped[...], cotan[kind, :, tile], preferred_element_type=jnp.float32)
-            target = pl.ds(pl.multiple_of(kind * cols + step * width_tile, width_tile), width_tile)
-            update_output[tokens : tokens + rank, target] = term
+    terms_of(theirs)
 
     far = others + (z,)
     for x_at in (1 - x, x):
@@ -501,7 +505,6 @@
     forward(*direction(fs), over_x)
     forward(direction(fs)[0], join_recv.at[0], over_core)
     cross(3, beside)
-    cross(2, across)
     piece_z(0, fs)
     second(3, x)
     piece_z(0, index(z, 1 - x, core))
@@ -510,6 +513,7 @@
         arrived(ref, sem)
         forward(ref, sem, over_x)
         forward(ref, join_recv.at[0], over_core)
+    cross(2, across)
     third(1, x)
     cross(1, mirror)
     from_x(1, beside, across)

time: 71.4 us -> 71.5 us (level)
  no operation moved by 1% of the time
where the time goes in v4:
time: 71.5 us; the launch traced here: 71.2 us
  Pallas kernels  70.5 us (99%)
    pallas_call x1, Pallas kernels, fused_body(): pl.pallas_call(functools.partial(fused, fs_size, tp_size), out_shape=[sha...  66.5 us
    pallas_call x1, Pallas kernels, fused_body(): pl.pallas_call(functools.partial(write, len(results)), out_shape=own + co...  4.06 us

profile of v4, /device:TPU:0, one launch (start us, length us, event | category | flops | bytes accessed | tf_op | source)
XLA Modules:
  0.0 71.2 jit_solution(14829879253679284477)
XLA Ops:
  0.6 66.5 %shard_map.195 = (f32[4,16,1024]{2,1,0:T(8,128)S(1)}, f32[128,1024]{1,0:T(8,128)S(1)}, f32[1024,128]{1,0:T(8,128)S(1)}, f32[128,1024]{1,0:T(8,128)S(1)}, f32[102...) custom-call(bf16[512,2048]{1,0:T(8,128)(2,1)} %input_hbm.1, ...), custom_call_target="tpu_custom_call" | custom-call | tf_op jit(solution)/shard_map/pallas_call | solution.py:660
  67.1 4.1 %shard_map.196 = (f32[128,1024]{1,0:T(8,128)}, f32[1024,128]{1,0:T(8,128)}, f32[128,1024]{1,0:T(8,128)}, f32[1024,128]{1,0:T(8,128)}, bf16[2048,1024]{1,0:T(8,12...) custom-call(f32[4,16,1024]{2,1,0:T(8,128)S(1)} %get-tuple-element.27, ...), custom_call_target="tpu_custom_call" | custom-call | tf_op jit(solution)/shard_map/pallas_call | solution.py:701
